TPU v7x, 512 devices: a whole 4x8x8 slice. The times are simulated.
512 devices in a mesh: gr: 2 (over z_hi), fs: 32 (over z_lo, y), tp: 8 (over x, core).
Axes of the slice: x: 4, y: 8, z: 8 (z_hi: 2, z_lo: 4; z = z_hi * 4 + z_lo), core: 2. Of those that a mesh axis runs over, the one named last changes fastest.
Arguments:
- prompt: bfloat16 [8192, 2048], P(('gr', 'fs')), may hold values from -6 to 6
- expert_ids: int32 [8192, 2], P(('gr', 'fs')), may hold values from 0 to 7, all different within a row; in each aligned block of 128 rows (0 to 127, 128 to 255, ...) at most 32 rows name the same one
- route_weights: float32 [8192, 2], P(('gr', 'fs')), may hold values from 0.2 to 1
- gate_master: float32 [8, 2048, 8192], P('gr', 'fs', 'tp'), may hold values from -0.125 to 0.125
- up_master: float32 [8, 2048, 8192], P('gr', 'fs', 'tp'), may hold values from -0.125 to 0.125
- down_master: float32 [8, 8192, 2048], P('gr', 'fs', 'tp'), may hold values from -0.0625 to 0.0625
- ffn_gain: float32 [2048], P('fs'), may hold values from 0.1 to 1.9
Outputs:
- gate_serving: bfloat16 [8, 2048, 8192], P('tp', None, 'fs')
- up_serving: bfloat16 [8, 2048, 8192], P('tp', None, 'fs')
- down_serving: bfloat16 [8, 8192, 2048], P('tp', 'fs')
- mixed: bfloat16 [8192, 2048], P(('gr', 'fs', 'tp'))
Inputs may be any that keep to these rules, and one draw needn't show every extreme that they name: `expert_ids`: the two experts of a token differ; the rows of one index of gr and fs name each expert exactly 32 times.
All inputs are finite; a program needn't handle non-finite values.
Results may differ from a plain program's by a relative error of at most 0.025.
Values may be sent and summed in bfloat16 or wider, within the bound.
A program may use at most 64 MiB of HBM per device.

v0:
```python
import jax
import jax.numpy as jnp
from jax import lax
from jax.sharding import Mesh
from jax.sharding import PartitionSpec as P

EXPERTS = 8
SLOTS = 32
FS = ("fs_0", "fs_1")
GR_FS = ("gr", "fs_0", "fs_1")
GR_FS_TP = ("gr", "fs_0", "fs_1", "tp")


NORM_EPS = 1e-06


def copy_for_each(value, axis):
    copies = jnp.broadcast_to(value, (lax.axis_size(axis), *value.shape))
    return lax.all_to_all(copies, axis, split_axis=0, concat_axis=0, tiled=True)


def in_order(parts, dim):
    parts = jnp.moveaxis(parts, 0, dim)
    dims = parts.shape
    return parts.reshape(*dims[:dim], dims[dim] * dims[dim + 1], *dims[dim + 2 :])


def gathered_copies(value, axis, dim):
    parts = copy_for_each(value, axis)
    return in_order(parts, dim)


def side_by_side(arrays, axis, dim, along):
    both = jnp.concatenate(arrays, axis=along)
    whole, at, finished = (gathered_copies(both, axis, dim), 0, [])
    for a in arrays:
        finished.append(lax.slice_in_dim(whole, at, at + a.shape[along], axis=along))
        at += a.shape[along]
    return tuple(finished)


def reduced_to_own(parts, axes, sequence):
    inside = parts.shape[1:]
    parts = parts.reshape(*(lax.axis_size(a) for a in axes), *inside)
    parts = jnp.moveaxis(parts, sequence, range(len(axes))).reshape(-1, *inside)
    for k in sequence:
        parts = lax.psum_scatter(parts, axes[k], scatter_dimension=0, tiled=True)
    return parts[0]


def in_blocks(value, dim, devices):
    before, after = (value.shape[:dim], value.shape[dim + 1 :])
    return jnp.moveaxis(value.reshape(*before, devices, -1, *after), dim, 0)


def scatter_axes(value, axes, sequence, dim):
    devices = lax.axis_size(axes)
    return reduced_to_own(in_blocks(value, dim, devices), axes, sequence)


def regroup_rows(weights, group_count, shard_count):
    local_experts, row_total, width = weights.shape
    stacked = weights.reshape(
        local_experts, group_count, shard_count, row_total // (group_count * shard_count), width
    )
    return stacked.transpose(0, 2, 1, 3, 4).reshape(local_experts, row_total, width)


def body(prompt, expert_ids, route_weights, gate_master, up_master, down_master, ffn_gain):
    group_count = lax.axis_size("gr")
    shard_count = lax.axis_size(FS)
    folding = ffn_gain[None, :, None]
    gate_local = (gate_master * folding).astype(jnp.bfloat16)
    up_local = (up_master * folding).astype(jnp.bfloat16)
    down_local = down_master.astype(jnp.bfloat16)
    gate_rows, up_rows = (
        lax.all_to_all(gate_local, "gr", split_axis=1, concat_axis=0, tiled=True),
        lax.all_to_all(up_local, "gr", split_axis=1, concat_axis=0, tiled=True),
    )
    down_whole = lax.all_gather(down_local, "gr", axis=0, tiled=True)
    gate_cols, up_cols = (
        lax.all_to_all(
            lax.all_to_all(gate_rows, "tp", split_axis=0, concat_axis=2, tiled=True),
            FS,
            split_axis=2,
            concat_axis=1,
            tiled=True,
        ),
        lax.all_to_all(
            lax.all_to_all(up_rows, "tp", split_axis=0, concat_axis=2, tiled=True),
            FS,
            split_axis=2,
            concat_axis=1,
            tiled=True,
        ),
    )
    down_serving = lax.all_to_all(down_whole, "tp", split_axis=0, concat_axis=2, tiled=True)
    gate_joined, up_joined = side_by_side((gate_cols, up_cols), "gr", 1, 0)
    gate_serving = regroup_rows(gate_joined, group_count, shard_count)
    up_serving = regroup_rows(up_joined, group_count, shard_count)
    token_count = prompt.shape[0]
    local_experts = gate_serving.shape[0]
    xfloat = prompt.astype(jnp.float32)
    normed = (
        xfloat * lax.rsqrt(jnp.mean(xfloat * xfloat, axis=1, keepdims=True) + NORM_EPS)
    ).astype(jnp.bfloat16)
    first_expert = lax.axis_index("tp") * local_experts
    pair_expert = expert_ids.reshape(-1)
    expert_table = (pair_expert[:, None] == jnp.arange(EXPERTS, dtype=jnp.int32)[None, :]).astype(
        jnp.int32
    )
    ranking = jnp.sum((jnp.cumsum(expert_table, axis=0) - expert_table) * expert_table, axis=1)
    local_ids = pair_expert - first_expert
    pair_token = jnp.arange(pair_expert.shape[0], dtype=jnp.int32) // 2
    matched = (
        local_ids[None, None, :] == jnp.arange(local_experts, dtype=jnp.int32)[:, None, None]
    ) & (ranking[None, None, :] == jnp.arange(SLOTS, dtype=jnp.int32)[None, :, None])
    slot_token = jnp.sum(jnp.where(matched, pair_token[None, None, :], 0), axis=2)
    filled = jnp.any(matched, axis=2)
    routed = jnp.where(filled[:, :, None], normed[slot_token], jnp.zeros((), jnp.bfloat16))
    piece = lax.all_gather(routed, FS, axis=1, tiled=True)
    gate_part = jnp.einsum("ecd,edf->ecf", piece, gate_serving, preferred_element_type=jnp.float32)
    up_part = jnp.einsum("ecd,edf->ecf", piece, up_serving, preferred_element_type=jnp.float32)
    hidden = (jax.nn.silu(gate_part) * up_part).astype(jnp.bfloat16)
    expert_out = scatter_axes(
        jnp.einsum("ecf,efd->ced", hidden, down_serving, preferred_element_type=jnp.float32).astype(
            jnp.bfloat16
        ),
        FS,
        (1, 0),
        0,
    ).astype(jnp.float32)
    is_local = (local_ids >= 0) & (local_ids < local_experts)
    safe_local = jnp.clip(local_ids, 0, local_experts - 1)
    safe_rank = jnp.minimum(ranking, SLOTS - 1)
    picked = expert_out[safe_rank, safe_local]
    weighted = jnp.where(
        is_local[:, None], picked * route_weights.reshape(-1)[:, None], 0.0
    ).astype(jnp.bfloat16)
    weighted = weighted.reshape(token_count, 2, weighted.shape[1])
    arrived = lax.all_to_all(weighted, "tp", split_axis=0, concat_axis=1, tiled=True)
    mixed = jnp.sum(arrived.astype(jnp.float32), axis=1).astype(jnp.bfloat16)
    return (gate_serving, up_serving, down_serving, mixed)


def solution(mesh):
    split = Mesh(
        mesh.devices.reshape(mesh.shape["gr"], 4, 8, mesh.shape["tp"]), ("gr", "fs_0", "fs_1", "tp")
    )
    placed = (
        P(GR_FS, None),
        P(GR_FS, None),
        P(GR_FS, None),
        P("gr", FS, "tp"),
        P("gr", FS, "tp"),
        P("gr", FS, "tp"),
        P(FS),
    )
    return jax.shard_map(
        body,
        mesh=split,
        in_specs=placed,
        out_specs=(P("tp", None, FS), P("tp", None, FS), P("tp", FS, None), P(GR_FS_TP, None)),
        check_vma=False,
    )
```

profile of v0, /device:TPU:1, one launch (start us, length us, event | category | flops | bytes accessed | tf_op | source)
XLA Modules:
  0.0 477.0 jit_solution(5518492747001386754)
XLA Ops:
  17.2 10.8 %all-to-all-start.3 = ((bf16[4,64,1024]{2,0,1:T(4,128)(2,1)}), bf16[4,64,1024]{2,0,1:T(4,128)(2,1)S(1)}, u32[]{:S(2)}, u32[]{:S(2)}) async-start(bf16[4,64,1024]{2,0,1:T(4,128)(2,1)} %copy.134), calls=%async_computation.3 | async-start | bytes 1048576 | tf_op jit(solution)/shard_map/all_to_all | solution.py:78
  29.2 10.5 %all-to-all-done.3 = bf16[4,64,1024]{2,0,1:T(4,128)(2,1)S(1)} async-done(((bf16[4,64,1024]{2,0,1:T(4,128)(2,1)}), bf16[4,64,1024]{2,0,1:T(4,128)(2,1)S(1)}, u32[]{:S(2)}, u32[]{:S(2)}) %all-to-all-start.3) | async-done | bytes 524320 | tf_op jit(solution)/shard_map/all_to_all | solution.py:78
  44.2 10.2 %all-to-all-done = bf16[4,64,1024]{2,0,1:T(4,128)(2,1)S(1)} async-done(((bf16[4,64,1024]{2,0,1:T(4,128)(2,1)}), bf16[4,64,1024]{2,0,1:T(4,128)(2,1)S(1)}, u32[]{:S(2)}, u32[]{:S(2)}) %all-to-all-start) | async-done | bytes 524320 | tf_op jit(solution)/shard_map/all_to_all | solution.py:77
  54.4 24.6 %all-to-all-start.4 = ((bf16[8,32,1024]{2,1,0:T(8,128)(2,1)}), bf16[8,32,1024]{2,1,0:T(8,128)(2,1)S(1)}, u32[]{:S(2)}, u32[]{:S(2)}) async-start(bf16[8,32,1024]{2,1,0:T(8,128)(2,1)} %bitcast.9), calls=%async_computation.4 | async-start | bytes 1048576 | tf_op jit(solution)/shard_map/all_to_all | solution.py:90
  80.0 8.3 %all-to-all-done.4 = bf16[8,32,1024]{2,1,0:T(8,128)(2,1)S(1)} async-done(((bf16[8,32,1024]{2,1,0:T(8,128)(2,1)}), bf16[8,32,1024]{2,1,0:T(8,128)(2,1)S(1)}, u32[]{:S(2)}, u32[]{:S(2)}) %all-to-all-start.4) | async-done | bytes 524320 | tf_op jit(solution)/shard_map/all_to_all | solution.py:90
  92.8 6.8 %copy.138 = bf16[1,32,8192]{1,0,2:T(2,128)(2,1)} copy(bf16[1,32,8192]{2,1,0:T(8,128)(2,1)S(1)} %bitcast.116) | data formatting | bytes 1048576 | tf_op jit(solution)/shard_map/all_to_all | solution.py:90
  100.0 45.2 %reduce.9 = bf16[8192,32]{1,0:T(8,128)(2,1)S(1)} reduce(bf16[8192,1,32]{2,1,0:T(2,128)(2,1)} %bitcast.105, bf16[]{:T(256)} %broadcast.353), dimensions={1}, to_apply=%bitcast.94.reduce_sub_computation | reduce | bytes 1048578
  148.0 18.7 %all-to-all-start.5 = ((bf16[32,2,4096]{2,1,0:T(2,128)(2,1)}), bf16[32,2,4096]{2,1,0:T(2,128)(2,1)S(1)}, u32[]{:S(2)}, u32[]{:S(2)}) async-start(bf16[32,2,4096]{2,1,0:T(2,128)(2,1)} %reshape.395), calls=%async_computation.5 | async-start | bytes 1048576 | tf_op jit(solution)/shard_map/all_to_all | solution.py:89
  166.7 6.8 %copy.131 = bf16[1,32,8192]{1,0,2:T(2,128)(2,1)} copy(bf16[1,32,8192]{2,1,0:T(8,128)(2,1)S(1)} %bitcast.117) | data formatting | bytes 1048576 | tf_op jit(solution)/shard_map/all_to_all | solution.py:83
  173.5 45.2 %reduce.10 = bf16[8192,32]{1,0:T(8,128)(2,1)S(1)} reduce(bf16[8192,1,32]{2,1,0:T(2,128)(2,1)} %bitcast.106, bf16[]{:T(256)} %broadcast.353), dimensions={1}, to_apply=%bitcast.96.reduce_sub_computation | reduce | bytes 1048578
  221.4 9.4 %all-to-all-start.2 = ((bf16[32,2,4096]{2,1,0:T(2,128)(2,1)}), bf16[32,2,4096]{2,1,0:T(2,128)(2,1)S(1)}, u32[]{:S(2)}, u32[]{:S(2)}) async-start(bf16[32,2,4096]{2,1,0:T(2,128)(2,1)} %reshape.397), calls=%async_computation.2 | async-start | bytes 1048576 | tf_op jit(solution)/shard_map/all_to_all | solution.py:82
  230.8 7.2 %reshape.396 = bf16[8192,1,32]{2,1,0:T(2,128)(2,1)} reshape(bf16[32,2,4096]{2,1,0:T(2,128)(2,1)S(1)} %all-to-all-done.5) | data formatting | bytes 1048576
  238.0 8.0 %copy.139 = bf16[1,32,8192]{2,1,0:T(8,128)(2,1)S(1)} copy(bf16[1,32,8192]{1,0,2:T(2,128)(2,1)} %bitcast.107) | data formatting | bytes 1048576 | tf_op jit(solution)/shard_map/all_to_all | solution.py:89
  246.4 7.2 %reshape.398 = bf16[8192,1,32]{2,1,0:T(2,128)(2,1)} reshape(bf16[32,2,4096]{2,1,0:T(2,128)(2,1)S(1)} %all-to-all-done.2) | data formatting | bytes 1048576
  253.6 8.0 %copy.132 = bf16[1,32,8192]{2,1,0:T(8,128)(2,1)S(1)} copy(bf16[1,32,8192]{1,0,2:T(2,128)(2,1)} %bitcast.108) | data formatting | bytes 1048576 | tf_op jit(solution)/shard_map/all_to_all | solution.py:82
  269.7 24.2 %all-to-all-done.6 = bf16[2,2,1024,256]{3,2,1,0:T(8,128)(2,1)S(1)} async-done(((bf16[2,2,1024,256]{3,2,1,0:T(8,128)(2,1)}), bf16[2,2,1024,256]{3,2,1,0:T(8,128)(2,1)S(1)}, u32[]{:S(2)}, u32[]{:S(2)}) %all-to-all-start.6) | async-done | bytes 2097184 | tf_op jit(solution)/shard_map/all_to_all | solution.py:19
  293.9 30.1 %all-to-all-start.7 = ((bf16[8,256,256]{1,2,0:T(8,128)(2,1)}), bf16[8,256,256]{1,2,0:T(8,128)(2,1)S(1)}, u32[]{:S(2)}, u32[]{:S(2)}) async-start(bf16[8,256,256]{1,2,0:T(8,128)(2,1)} %copy.144), calls=%async_computation.7 | async-start | bytes 2097152 | tf_op jit(solution)/shard_map/all_to_all | solution.py:97
  324.5 5.1 %fusion.2 = f32[1024,256]{1,0:T(8,128)} fusion(bf16[2048,256]{1,0:T(8,128)(2,1)S(1)} %bitcast.129, bf16[1,1024,2048]{2,1,0:T(8,128)(2,1)} %all-gather.5.cloned.1.call-done), kind=kOutput, calls=%fused_computation.4 | convolution fusion | flops 1073741824 | bytes 6291456 | tf_op jit(solution)/shard_map/ecd,edf->ecf/dot_general | solution.py:122
  329.6 9.3 %all-to-all-done.7 = bf16[8,256,256]{1,2,0:T(8,128)(2,1)S(1)} async-done(((bf16[8,256,256]{1,2,0:T(8,128)(2,1)}), bf16[8,256,256]{1,2,0:T(8,128)(2,1)S(1)}, u32[]{:S(2)}, u32[]{:S(2)}) %all-to-all-start.7) | async-done | bytes 1048608 | tf_op jit(solution)/shard_map/all_to_all | solution.py:97
  339.0 8.8 %convolution_convert_fusion = bf16[1024,2048]{1,0:T(8,128)(2,1)} fusion(bf16[256,2048]{0,1:T(8,128)(2,1)S(1)} %bitcast.112, bf16[2048,256]{1,0:T(8,128)(2,1)S(1)} %bitcast.131, bf16[1,1024,2048]{2,1,0:T(8,128)(2,1)} %all-gather.5.cloned.1.call-done, f32[1024,256]{1,0:T(8,128)} %fusion.2), kind=kOutput, calls=%fused_computation.6 | convolution fusion | flops 2151153664 | bytes 11534336 | tf_op jit(solution)/shard_map/ecf,efd->ced/dot_general | solution.py:126
  352.5 53.6 %reduce-scatter.3.cloned.1.call-done = bf16[4,32,1,2048]{3,1,2,0:T(8,128)(2,1)} async-done(((bf16[32,32,1,2048]{3,1,2,0:T(8,128)(2,1)}), bf16[4,32,1,2048]{3,1,2,0:T(8,128)(2,1)}) %reduce-scatter.3.cloned.1.call-update) | async-done | bytes 524304 | tf_op jit(solution)/shard_map/reduce_scatter | solution.py:47
  406.7 29.8 %reduce-scatter.5.cloned.1.call-done = bf16[1,32,1,2048]{3,1,2,0:T(8,128)(2,1)} async-done(((bf16[4,32,1,2048]{3,1,2,0:T(8,128)(2,1)}), bf16[1,32,1,2048]{3,1,2,0:T(8,128)(2,1)}) %reduce-scatter.5.cloned.1.call-update) | async-done | bytes 131088 | tf_op jit(solution)/shard_map/reduce_scatter | solution.py:47
  445.4 6.5 %all-to-all-start.8 = ((bf16[128,2,2048]{2,1,0:T(2,128)(2,1)}), bf16[128,2,2048]{2,1,0:T(2,128)(2,1)S(1)}, u32[]{:S(2)}, u32[]{:S(2)}) async-start(bf16[128,2,2048]{2,1,0:T(2,128)(2,1)} %select_convert_fusion), calls=%async_computation.10 | async-start | bytes 2097152 | tf_op jit(solution)/shard_map/all_to_all | solution.py:141
  453.3 13.6 %all-to-all-done.8 = bf16[128,2,2048]{2,1,0:T(2,128)(2,1)S(1)} async-done(((bf16[128,2,2048]{2,1,0:T(2,128)(2,1)}), bf16[128,2,2048]{2,1,0:T(2,128)(2,1)S(1)}, u32[]{:S(2)}, u32[]{:S(2)}) %all-to-all-start.8) | async-done | bytes 1048608 | tf_op jit(solution)/shard_map/all_to_all | solution.py:141
  (92 shorter events, 55.1 us)
Async XLA Ops:
  7.2 8.5 %copy-start = (f32[4,64,1024]{2,1,0:T(8,128)S(1)}, f32[4,64,1024]{2,1,0:T(8,128)}, u32[]{:S(2)}) copy-start(f32[4,64,1024]{2,1,0:T(8,128)} %param.10) | copy-start | bytes 3145732
  7.2 8.5 %copy-start.1 = (f32[4,64,1024]{2,1,0:T(8,128)S(1)}, f32[4,64,1024]{2,1,0:T(8,128)}, u32[]{:S(2)}) copy-start(f32[4,64,1024]{2,1,0:T(8,128)} %param.11) | copy-start | bytes 3145732
  7.2 8.5 %copy-start.6 = (f32[64]{0:T(128)S(1)}, f32[64]{0:T(128)}, u32[]{:S(2)}) copy-start(f32[64]{0:T(128)} %param.13) | copy-start | bytes 772
  7.2 260.2 %all-gather.3.cloned.1.call-start = ((), (), s32[]{:S(2)}) async-start(), calls=%async_computation.11 | async-start | bytes 1572864 | tf_op jit(solution)/shard_map/all_gather | solution.py:80
  9.5 315.0 %all-gather.5.cloned.1.call-start = ((), (), s32[]{:S(2)}) async-start(), calls=%async_computation.12 | async-start | bytes 4325376 | tf_op jit(solution)/shard_map/all_gather | solution.py:121
  17.2 22.5 %all-to-all-start.3 = ((bf16[4,64,1024]{2,0,1:T(4,128)(2,1)}), bf16[4,64,1024]{2,0,1:T(4,128)(2,1)S(1)}, u32[]{:S(2)}, u32[]{:S(2)}) async-start(bf16[4,64,1024]{2,0,1:T(4,128)(2,1)} %copy.134), calls=%async_computation.3 | async-start | bytes 1048576 | tf_op jit(solution)/shard_map/all_to_all | solution.py:78
  39.7 14.7 %all-to-all-start = ((bf16[4,64,1024]{2,0,1:T(4,128)(2,1)}), bf16[4,64,1024]{2,0,1:T(4,128)(2,1)S(1)}, u32[]{:S(2)}, u32[]{:S(2)}) async-start(bf16[4,64,1024]{2,0,1:T(4,128)(2,1)} %copy.127), calls=%async_computation | async-start | bytes 1048576 | tf_op jit(solution)/shard_map/all_to_all | solution.py:77
  54.4 34.0 %all-to-all-start.4 = ((bf16[8,32,1024]{2,1,0:T(8,128)(2,1)}), bf16[8,32,1024]{2,1,0:T(8,128)(2,1)S(1)}, u32[]{:S(2)}, u32[]{:S(2)}) async-start(bf16[8,32,1024]{2,1,0:T(8,128)(2,1)} %bitcast.9), calls=%async_computation.4 | async-start | bytes 1048576 | tf_op jit(solution)/shard_map/all_to_all | solution.py:90
  88.4 59.6 %all-to-all-start.1 = ((bf16[8,32,1024]{2,1,0:T(8,128)(2,1)}), bf16[8,32,1024]{2,1,0:T(8,128)(2,1)S(1)}, u32[]{:S(2)}, u32[]{:S(2)}) async-start(bf16[8,32,1024]{2,1,0:T(8,128)(2,1)} %bitcast.2), calls=%async_computation.1 | async-start | bytes 1048576 | tf_op jit(solution)/shard_map/all_to_all | solution.py:83
  148.0 73.4 %all-to-all-start.5 = ((bf16[32,2,4096]{2,1,0:T(2,128)(2,1)}), bf16[32,2,4096]{2,1,0:T(2,128)(2,1)S(1)}, u32[]{:S(2)}, u32[]{:S(2)}) async-start(bf16[32,2,4096]{2,1,0:T(2,128)(2,1)} %reshape.395), calls=%async_computation.5 | async-start | bytes 1048576 | tf_op jit(solution)/shard_map/all_to_all | solution.py:89
  221.4 25.0 %all-to-all-start.2 = ((bf16[32,2,4096]{2,1,0:T(2,128)(2,1)}), bf16[32,2,4096]{2,1,0:T(2,128)(2,1)S(1)}, u32[]{:S(2)}, u32[]{:S(2)}) async-start(bf16[32,2,4096]{2,1,0:T(2,128)(2,1)} %reshape.397), calls=%async_computation.2 | async-start | bytes 1048576 | tf_op jit(solution)/shard_map/all_to_all | solution.py:82
  263.6 30.3 %all-to-all-start.6 = ((bf16[2,2,1024,256]{3,2,1,0:T(8,128)(2,1)}), bf16[2,2,1024,256]{3,2,1,0:T(8,128)(2,1)S(1)}, u32[]{:S(2)}, u32[]{:S(2)}) async-start(bf16[2,2,1024,256]{3,2,1,0:T(8,128)(2,1)} %broadcast_in_dim.51), calls=%async_computation.6 | async-start | bytes 4194304 | tf_op jit(solution)/shard_map/all_to_all | solution.py:19
  293.9 45.1 %all-to-all-start.7 = ((bf16[8,256,256]{1,2,0:T(8,128)(2,1)}), bf16[8,256,256]{1,2,0:T(8,128)(2,1)S(1)}, u32[]{:S(2)}, u32[]{:S(2)}) async-start(bf16[8,256,256]{1,2,0:T(8,128)(2,1)} %copy.144), calls=%async_computation.7 | async-start | bytes 2097152 | tf_op jit(solution)/shard_map/all_to_all | solution.py:97
  324.0 82.1 %reduce-scatter.3.cloned.1.call-start = ((), (), s32[]{:S(2)}) async-start(), calls=%async_computation.13 | async-start | bytes 4718592 | tf_op jit(solution)/shard_map/reduce_scatter | solution.py:47
  324.4 5.3 %copy-start.2 = (bf16[1,32,2,32,256]{4,3,2,1,0:T(8,128)(2,1)}, bf16[1,32,2,32,256]{4,3,2,1,0:T(8,128)(2,1)S(1)}, u32[]{:S(2)}) copy-start(bf16[1,32,2,32,256]{4,3,2,1,0:T(8,128)(2,1)S(1)} %copy.142) | copy-start | bytes 3145732
  324.4 23.3 %copy-start.3 = (bf16[1,32,2,32,256]{4,3,2,1,0:T(8,128)(2,1)}, bf16[1,32,2,32,256]{4,3,2,1,0:T(8,128)(2,1)S(1)}, u32[]{:S(2)}) copy-start(bf16[1,32,2,32,256]{4,3,2,1,0:T(8,128)(2,1)S(1)} %copy.143) | copy-start | bytes 3145732
  352.5 53.7 %copy-start.4 = (s32[128,2]{0,1:T(2,128)S(1)}, s32[128,2]{0,1:T(2,128)}, u32[]{:S(2)}) copy-start(s32[128,2]{0,1:T(2,128)} %param.8) | copy-start | bytes 3076
  352.5 54.1 %copy-start.5 = (f32[128,2]{0,1:T(2,128)S(1)}, f32[128,2]{0,1:T(2,128)}, u32[]{:S(2)}) copy-start(f32[128,2]{0,1:T(2,128)} %param.9) | copy-start | bytes 3076
  352.5 84.0 %reduce-scatter.5.cloned.1.call-start = ((), (), s32[]{:S(2)}) async-start(), calls=%async_computation.14 | async-start | bytes 655360 | tf_op jit(solution)/shard_map/reduce_scatter | solution.py:47
  445.4 21.4 %all-to-all-start.8 = ((bf16[128,2,2048]{2,1,0:T(2,128)(2,1)}), bf16[128,2,2048]{2,1,0:T(2,128)(2,1)S(1)}, u32[]{:S(2)}, u32[]{:S(2)}) async-start(bf16[128,2,2048]{2,1,0:T(2,128)(2,1)} %select_convert_fusion), calls=%async_computation.10 | async-start | bytes 2097152 | tf_op jit(solution)/shard_map/all_to_all | solution.py:141
Sparse Core Ops, SparseCore 0:
  10.7 42.0 all-gather.2
  54.9 166.2 all-gather.4
  352.6 53.4 reduce-scatter.2
  408.8 27.6 reduce-scatter.4
where the time goes:
time: 478 us; the launch traced here: 477 us
  waiting for transfers between devices  160 us (33%)
  starting transfers between devices  112 us (23%)
  other arithmetic  105 us (22%)
  local copies, waits for them, and re-layouts  72.5 us (15%)
  between operations  14.1 us (3%)
  matrix products  13.9 us (3%)
    unnamed x2, other arithmetic  90.4 us
    reduce_scatter x2, waiting for transfers between devices, reduced_to_own(): parts = lax.psum_scatter(parts, axes[k], scatter_dimension=0, tiled=True)  83.4 us
    all_to_all x1, starting transfers between devices, body(): lax.all_to_all(down_whole, 'tp', split_axis=0, concat_axis=2, tiled=True)  30.1 us
    all_to_all x1, starting transfers between devices, body(): lax.all_to_all(up_rows, 'tp', split_axis=0, concat_axis=2, tiled=True)  24.6 us
    all_to_all x1, waiting for transfers between devices, copy_for_each(): return lax.all_to_all(copies, axis, split_axis=0, concat_axis=0, tiled=True)  24.2 us
    unnamed x24, local copies, waits for them, and re-layouts  22.9 us
    all_to_all x1, starting transfers between devices, body(): lax.all_to_all(lax.all_to_all(up_rows, 'tp', split_axis=0, concat_axis=2,...  18.7 us
    all_to_all x1, waiting for transfers between devices, body(): lax.all_to_all(weighted, 'tp', split_axis=0, concat_axis=1, tiled=True)  13.6 us
  transfers between devices with their start and end apart: 13, of which 8 were waited for; matrix products, arithmetic and copies ran while one was open for 34% of the time, Pallas kernels for 0%

commit v1 on v0

v1 whole, which is shorter than its diff:
```python
import functools

import jax
import jax.numpy as jnp
from jax import lax
from jax.experimental import pallas as pl
from jax.experimental.pallas import tpu as pltpu
from jax.sharding import PartitionSpec as P

EXPERTS = 8
SLOTS = 32
TOK = 128
D = 2048
NORM_EPS = 1e-06
MESH = pl.DeviceIdType.MESH
BF = jnp.bfloat16
F32 = jnp.float32


def place():
    g, f, t = lax.axis_index("gr"), lax.axis_index("fs"), lax.axis_index("tp")
    return g, lax.div(f, 8), lax.rem(f, 8), lax.div(t, 2), lax.rem(t, 2)


def dev(g, zl, y, x, c):
    return (g, zl * 8 + y, x * 2 + c)


def signal(sem, where):
    pl.semaphore_signal(sem, inc=1, device_id=where, device_id_type=MESH)


def rcopy(src, dst, ssem, rsem, where):
    return pltpu.make_async_remote_copy(
        src_ref=src, dst_ref=dst, send_sem=ssem, recv_sem=rsem, device_id=where, device_id_type=MESH
    )


def arrived(buf, sem):
    pltpu.make_async_copy(buf, buf, sem).wait()


def home_of(g, el):
    odd = lax.rem(el, 2)
    x1 = 2 * g + lax.div(el, 2)
    return x1, odd, x1 * (1 - odd) + (3 - x1) * odd


def served_by(g, x):
    h = lax.div(x, 2)
    c1 = h + g - 2 * h * g
    return x * (1 - c1) + (3 - x) * c1, c1


def choice_matrix(ids):
    e = lax.axis_index("tp")
    hit = (ids == e).astype(F32)
    mine = jnp.sum(hit, axis=1, keepdims=True)
    mine = jnp.broadcast_to(mine, (TOK, SLOTS))
    row = lax.broadcasted_iota(jnp.int32, (TOK, TOK), 0)
    col = lax.broadcasted_iota(jnp.int32, (TOK, TOK), 1)
    before = (col < row).astype(BF)
    rank = jnp.dot(before, mine.astype(BF), preferred_element_type=F32)
    slot = lax.broadcasted_iota(jnp.int32, (TOK, SLOTS), 1).astype(F32)
    return jnp.where((mine > 0.5) & (jnp.abs(rank - slot) < 0.5), 1.0, 0.0)


def gather_kernel(
    prompt, ids, gain, gate, up, down,
    gate_out, up_out, down_out, rows,
    stg, stgd, abuf, dbuf,
    a_s, a_r, d_s, d_r, b_s, b_r, e_s, e_r, t_s, t_r, y_s, y_r,
):
    g, zl, y, x, c = place()
    me_t = x * 2 + c
    barrier = pltpu.get_barrier_semaphore()
    right = dev(g, zl, lax.rem(y + 1, 8), x, c)
    left = dev(g, zl, lax.rem(y + 7, 8), x, c)
    half = lax.div(y, 4)
    x1, c1 = served_by(g, x)
    ge = lax.div(x, 2)
    _, _, xe = home_of(ge, lax.rem(me_t, 4))

    @pl.loop(0, 32)
    def _(i):
        xs, ys = lax.div(i, 8), lax.rem(i, 8)

        @pl.when((xs != x) | (ys != y) | (half != c))
        def _():
            signal(barrier, dev(g, zl, ys, xs, half))

    @pl.loop(0, 8)
    def _(i):
        @pl.when(i != me_t)
        def _():
            signal(barrier, (g, zl * 8 + y, i))

        zs, w = lax.div(i, 2), lax.rem(i, 2)

        @pl.when((ge != g) | (zs != zl) | (xe != x) | (w != c))
        def _():
            signal(barrier, dev(ge, zs, y, xe, w))

    @pl.loop(1, 4)
    def _(j):
        signal(barrier, dev(g, lax.rem(zl + j, 4), y, x, c))

    signal(barrier, right)
    signal(barrier, left)

    chosen = choice_matrix(ids[...]).astype(BF)
    xf = prompt[...].astype(F32)
    normed = (xf * lax.rsqrt(jnp.mean(xf * xf, axis=1, keepdims=True) + NORM_EPS)).astype(BF)
    routed = lax.dot_general(chosen, normed, (((0,), (0,)), ((), ())), preferred_element_type=F32)
    rows[y, zl] = routed.astype(BF)

    @pl.loop(0, 4)
    def _(el):
        for h in range(2):
            stgd[el, h] = down[el, h * 128 : (h + 1) * 128, :].astype(BF)

    col = gain[...]

    @pl.loop(0, 4)
    def _(el):
        for k in range(4):
            cols = slice(k * 256, (k + 1) * 256)
            stg[0, el, k] = (gate[el, :, cols] * col).astype(BF)
            stg[1, el, k] = (up[el, :, cols] * col).astype(BF)

    same_half = jnp.where(half == c, 1, 0)
    own_b = jnp.where(ge == g, 1, 0) * (1 - c)
    pl.semaphore_wait(barrier, 32 - same_half + 7 + 8 - own_b + 3 + 2)

    def z_send(j):
        to = lax.rem(zl + j, 4)
        return rcopy(rows.at[y, zl], rows.at[y, zl], t_s.at[j], t_r.at[zl], dev(g, to, y, x, c))

    def r_send(s, q):
        at = lax.rem(y - s + 9, 8)
        return rcopy(rows.at[at, q], rows.at[at, q], y_s.at[0, s, q], y_r.at[0, s, q], right)

    def l_send(s, q):
        at = lax.rem(y + s + 7, 8)
        return rcopy(rows.at[at, q], rows.at[at, q], y_s.at[1, s, q], y_r.at[1, s, q], left)

    @pl.loop(1, 4)
    def _(j):
        z_send(j).start()

    def d_parts(i):
        el, h = lax.div(i, 2), lax.rem(i, 2)
        _, _, x2 = home_of(g, el)
        own = (x2 == x) & (h == c)
        dst = dbuf.at[:, pl.ds(pl.multiple_of(me_t * 256, 256), 256)]
        return own, stgd.at[el, h], dst, dev(g, zl, y, x2, h)

    @pl.loop(0, 8)
    def _(i):
        own, src, dst, to = d_parts(i)

        @pl.when(own)
        def _():
            pltpu.make_async_copy(src, dst, d_r).start()

        @pl.when(jnp.logical_not(own))
        def _():
            rcopy(src, dst, d_s.at[i], d_r, to).start()

    r_send(1, zl).start()
    l_send(1, zl).start()

    def a_parts(i):
        el, k, w = lax.div(i, 8), lax.rem(lax.div(i, 2), 4), lax.rem(i, 2)
        _, _, x2 = home_of(g, el)
        y2 = 4 * c + k
        own = (x2 == x) & (w == c) & (y2 == y)
        dst = abuf.at[x, pl.ds(pl.multiple_of(y * 64, 64), 64), :]
        return own, stg.at[w, el, k], dst, dev(g, zl, y2, x2, w)

    @pl.loop(0, 32)
    def _(i):
        own, src, dst, to = a_parts(i)

        @pl.when(own)
        def _():
            pltpu.make_async_copy(src, dst, a_r.at[x]).start()

        @pl.when(jnp.logical_not(own))
        def _():
            rcopy(src, dst, a_s.at[i], a_r.at[x], to).start()

    def e_parts(i):
        g2 = lax.rem(g + i, 2)
        own = (i == 0) & (x1 == x) & (c1 == c)
        dst = down_out.at[pl.ds(pl.multiple_of(c * 128, 128), 128), :]
        return own, dbuf, dst, dev(g2, zl, y, x1, c1)

    arrived(dbuf, d_r)

    @pl.loop(0, 2)
    def _(i):
        own, src, dst, to = e_parts(i)

        @pl.when(own)
        def _():
            pltpu.make_async_copy(src, dst, e_r.at[c]).start()

        @pl.when(jnp.logical_not(own))
        def _():
            rcopy(src, dst, e_s.at[i], e_r.at[c], to).start()

    @pl.loop(1, 4)
    def _(j):
        q = lax.rem(zl + j, 4)
        arrived(rows.at[y, q], t_r.at[q])
        r_send(1, q).start()
        l_send(1, q).start()

    def b_parts(i, out):
        xs, g2 = lax.div(i, 2), lax.rem(i, 2)
        own = (g2 == g) & (xs == zl) & (x1 == x) & (c1 == c)
        dst = out.at[pl.ds(pl.multiple_of(zl * 512, 512), 512), :]
        return own, abuf.at[xs], dst, dev(g2, xs, y, x1, c1)

    for w, out in ((0, gate_out), (1, up_out)):

        @pl.when(c == w)
        def _():
            @pl.loop(0, 8)
            def _(i):
                own, src, dst, to = b_parts(i, out)

                @pl.when(lax.rem(i, 2) == 0)
                def _():
                    arrived(src, a_r.at[lax.div(i, 2)])

                @pl.when(own)
                def _():
                    pltpu.make_async_copy(src, dst, b_r.at[w, zl]).start()

                @pl.when(jnp.logical_not(own))
                def _():
                    rcopy(src, dst, b_s.at[i], b_r.at[w, zl], to).start()

    def ring_step(s):
        @pl.loop(0, 4)
        def _(j):
            q = lax.rem(zl + j, 4)
            arrived(rows.at[lax.rem(y - s + 9, 8), q], y_r.at[0, s - 1, q])
            arrived(rows.at[lax.rem(y + s + 7, 8), q], y_r.at[1, s - 1, q])
            if s < 4:
                r_send(s, q).start()
                l_send(s, q).start()
            else:

                @pl.when(q < 2)
                def _():
                    r_send(s, q).start()

                @pl.when(q >= 2)
                def _():
                    l_send(s, q).start()

    for s in (2, 3, 4):
        ring_step(s)

    far = lax.rem(y + 4, 8)
    for q in range(4):
        arrived(rows.at[far, q], y_r.at[q // 2, 4, q])
    for q in range(4):
        arrived(gate_out.at[q * 512 : (q + 1) * 512, :], b_r.at[0, q])
        arrived(up_out.at[q * 512 : (q + 1) * 512, :], b_r.at[1, q])
    for h in range(2):
        arrived(down_out.at[h * 128 : (h + 1) * 128, :], e_r.at[h])

    @pl.loop(1, 4)
    def _(j):
        z_send(j).wait_send()

    @pl.loop(0, 8)
    def _(i):
        own, src, dst, to = d_parts(i)

        @pl.when(jnp.logical_not(own))
        def _():
            rcopy(src, dst, d_s.at[i], d_r, to).wait_send()

    @pl.loop(0, 32)
    def _(i):
        own, src, dst, to = a_parts(i)

        @pl.when(jnp.logical_not(own))
        def _():
            rcopy(src, dst, a_s.at[i], a_r.at[x], to).wait_send()

    @pl.loop(0, 2)
    def _(i):
        own, src, dst, to = e_parts(i)

        @pl.when(jnp.logical_not(own))
        def _():
            rcopy(src, dst, e_s.at[i], e_r.at[c], to).wait_send()

    @pl.loop(0, 8)
    def _(i):
        own, src, dst, to = b_parts(i, gate_out)

        @pl.when(jnp.logical_not(own))
        def _():
            rcopy(src, dst, b_s.at[i], b_r.at[0, zl], to).wait_send()

    for s in (1, 2, 3):

        @pl.loop(0, 4)
        def _(q):
            r_send(s, q).wait_send()
            l_send(s, q).wait_send()

    for q in range(2):
        r_send(4, q).wait_send()
        l_send(4, q + 2).wait_send()


def combine_kernel(
    part, ids, weights, mixed,
    keep, got, fin, gotz, sendc, gotc,
    y_s, y_r, z_s, z_r, c_s, c_r,
):
    g, zl, y, x, c = place()
    me_t = x * 2 + c
    barrier = pltpu.get_barrier_semaphore()
    right = dev(g, zl, lax.rem(y + 1, 8), x, c)
    left = dev(g, zl, lax.rem(y + 7, 8), x, c)
    signal(barrier, right)
    signal(barrier, left)

    @pl.loop(1, 4)
    def _(j):
        signal(barrier, dev(g, lax.rem(zl + j, 4), y, x, c))

    @pl.loop(1, 8)
    def _(j):
        signal(barrier, (g, zl * 8 + y, lax.rem(me_t + j, 8)))

    chosen = choice_matrix(ids[...])
    e = lax.axis_index("tp")
    wcol = jnp.sum(jnp.where(ids[...] == e, weights[...], 0.0), axis=1, keepdims=True)
    wrow = jnp.sum(chosen * wcol, axis=0, keepdims=True)
    eye = lax.broadcasted_iota(jnp.int32, (SLOTS, SLOTS), 0) == lax.broadcasted_iota(
        jnp.int32, (SLOTS, SLOTS), 1
    )
    wslot = jnp.sum(jnp.where(eye, jnp.broadcast_to(wrow, (SLOTS, SLOTS)), 0.0), axis=1, keepdims=True)

    pl.semaphore_wait(barrier, 12)

    def target(way, s):
        return lax.rem(y + 5 - s, 8) if way == 0 else lax.rem(y + 3 + s, 8)

    def send(way, s, q, src):
        return rcopy(
            src, got.at[way, s - 1, q], y_s.at[way, s - 1, q], y_r.at[way, s - 1, q], (right, left)[way]
        )

    def first_hand(way, s, q):
        return s == 1 or (s == 2 and q // 2 != way)

    def source(way, s, q):
        if first_hand(way, s, q):
            return part.at[target(way, s), q]
        return keep.at[way, s - 2, q]

    for q in range(2):
        for way in range(2):
            send(way, 1, q + 2 * way, source(way, 1, q + 2 * way)).start()
    for q in range(2):
        for way in range(2):
            other = q + 2 * (1 - way)
            send(way, 2, other, source(way, 2, other)).start()
    for s in (2, 3, 4):
        order = (0, 1) if s == 2 else (2, 3, 0, 1)
        for j in order:
            for way in range(2):
                q = (j + 2 * way) % 4
                arrived(got.at[way, s - 2, q], y_r.at[way, s - 2, q])
                total = part[target(way, s), q].astype(F32) + got[way, s - 2, q].astype(F32)
                keep[way, s - 2, q] = total.astype(BF)
                send(way, s, q, source(way, s, q)).start()

    def z_send(q):
        return rcopy(fin.at[q], gotz.at[zl], z_s.at[q], z_r.at[zl], dev(g, q, y, x, c))

    for q in (2, 0, 3, 1):
        for way in range(2):
            arrived(got.at[way, 3, q], y_r.at[way, 3, q])
        total = part[y, q].astype(F32) + got[0, 3, q].astype(F32) + got[1, 3, q].astype(F32)
        fin[q] = total.astype(BF)

        @pl.when(zl != q)
        def _():
            z_send(q).start()

    out = fin[zl].astype(F32)
    for j in range(1, 4):
        q = lax.rem(zl + j, 4)
        arrived(gotz.at[q], z_r.at[q])
        out = out + gotz[q].astype(F32)

    term = (out * wslot).astype(BF)
    spread = jnp.dot(chosen.astype(BF), term, preferred_element_type=F32).astype(BF)
    for t in range(8):
        sendc[t] = spread[t * 16 : (t + 1) * 16, :]

    def c_send(j):
        t = lax.rem(me_t + j, 8)
        return rcopy(sendc.at[t], gotc.at[me_t], c_s.at[j], c_r.at[me_t], (g, zl * 8 + y, t))

    @pl.loop(1, 8)
    def _(j):
        c_send(j).start()

    total = sendc[me_t].astype(F32)
    for j in range(1, 8):
        t = lax.rem(me_t + j, 8)
        arrived(gotc.at[t], c_r.at[t])
        total = total + gotc[t].astype(F32)
    mixed[...] = total.astype(BF)

    for s in (1, 2, 3, 4):
        for q in range(4):
            for way in range(2):
                if s > 1 or q // 2 == way:
                    send(way, s, q, source(way, s, q)).wait_send()
    for q in range(4):

        @pl.when(zl != q)
        def _():
            z_send(q).wait_send()

    @pl.loop(1, 8)
    def _(j):
        c_send(j).wait_send()


VM = pl.BlockSpec(memory_space=pltpu.VMEM)
DMA = pltpu.SemaphoreType.DMA


def body(prompt, expert_ids, route_weights, gate_master, up_master, down_master, ffn_gain):
    gate, up, down, rows = pl.pallas_call(
        gather_kernel,
        out_shape=(
            jax.ShapeDtypeStruct((D, 256), BF),
            jax.ShapeDtypeStruct((D, 256), BF),
            jax.ShapeDtypeStruct((256, D), BF),
            jax.ShapeDtypeStruct((8, 4, SLOTS, D), BF),
        ),
        in_specs=[VM] * 6,
        out_specs=(VM,) * 4,
        scratch_shapes=[
            pltpu.VMEM((2, 4, 4, 64, 256), BF),
            pltpu.VMEM((4, 2, 128, 256), BF),
            pltpu.VMEM((4, 512, 256), BF),
            pltpu.VMEM((128, D), BF),
            DMA((32,)),
            DMA((4,)),
            DMA((8,)),
            DMA,
            DMA((8,)),
            DMA((2, 4)),
            DMA((2,)),
            DMA((2,)),
            DMA((4,)),
            DMA((4,)),
            DMA((2, 5, 4)),
            DMA((2, 5, 4)),
        ],
        compiler_params=pltpu.CompilerParams(
            collective_id=0, has_side_effects=True, vmem_limit_bytes=40 << 20
        ),
        name="gather",
    )(prompt, expert_ids, ffn_gain[:, None], gate_master, up_master, down_master)
    piece = rows.reshape(8 * 4 * SLOTS, D)
    gate_part = jnp.dot(piece, gate, preferred_element_type=F32)
    up_part = jnp.dot(piece, up, preferred_element_type=F32)
    hidden = (jax.nn.silu(gate_part) * up_part).astype(BF)
    part = jnp.dot(hidden, down, preferred_element_type=F32).astype(BF)
    mixed = pl.pallas_call(
        combine_kernel,
        out_shape=jax.ShapeDtypeStruct((16, D), BF),
        in_specs=[VM] * 3,
        out_specs=VM,
        scratch_shapes=[
            pltpu.VMEM((2, 3, 4, SLOTS, D), BF),
            pltpu.VMEM((2, 4, 4, SLOTS, D), BF),
            pltpu.VMEM((4, SLOTS, D), BF),
            pltpu.VMEM((4, SLOTS, D), BF),
            pltpu.VMEM((8, 16, D), BF),
            pltpu.VMEM((8, 16, D), BF),
            DMA((2, 4, 4)),
            DMA((2, 4, 4)),
            DMA((4,)),
            DMA((4,)),
            DMA((8,)),
            DMA((8,)),
        ],
        compiler_params=pltpu.CompilerParams(
            collective_id=1, has_side_effects=True, vmem_limit_bytes=40 << 20
        ),
        name="combine",
    )(part.reshape(8, 4, SLOTS, D), expert_ids, route_weights)
    return gate[None], up[None], down[None], mixed


def solution(mesh):
    return jax.shard_map(
        body,
        mesh=mesh,
        in_specs=(
            P(("gr", "fs"), None),
            P(("gr", "fs"), None),
            P(("gr", "fs"), None),
            P("gr", "fs", "tp"),
            P("gr", "fs", "tp"),
            P("gr", "fs", "tp"),
            P("fs"),
        ),
        out_specs=(
            P("tp", None, "fs"),
            P("tp", None, "fs"),
            P("tp", "fs", None),
            P(("gr", "fs", "tp"), None),
        ),
        check_vma=False,
    )
```

time: 478 us -> 198 us (0.41)
  Pallas kernels: 0 us -> 169 us
  waiting for transfers between devices: 160 us -> 0 us
  starting transfers between devices: 112 us -> 0 us
  other arithmetic: 105 us -> 0 us
  local copies, waits for them, and re-layouts: 72.5 us -> 14 us
  between operations: 14.1 us -> 0.67 us
    pallas_call x0 -> x2, Pallas kernels: none -> 169 us  [the longest x1 89.7 us: body(): pl.pallas_call(combine_kernel, out_shape=jax.ShapeDtypeStruct((16, D), BF...]
    all_to_all x9 -> x0, starting transfers between devices: 112 us -> none  [the longest x1 30.1 us: body(): lax.all_to_all(down_whole, 'tp', split_axis=0, concat_axis=2, tiled=True)]
    unnamed x2 -> x0, other arithmetic: 90.4 us -> none
    reduce_scatter x2 -> x0, waiting for transfers between devices: 83.4 us -> none  [reduced_to_own(): parts = lax.psum_scatter(parts, axes[k], scatter_dimension=0, tiled=True)]
    all_to_all x9 -> x0, waiting for transfers between devices: 76.1 us -> none  [the longest x1 24.2 us: copy_for_each(): return lax.all_to_all(copies, axis, split_axis=0, concat_axis=0, tiled=True)]
    all_to_all x15 -> x0, local copies, waits for them, and re-layouts: 32.3 us -> none  [the longest x3 8.3 us: body(): lax.all_to_all(lax.all_to_all(up_rows, 'tp', split_axis=0, concat_axis=2,...]
    unnamed x24 -> x20, local copies, waits for them, and re-layouts: 22.9 us -> 13.3 us
    convert_element_type x6 -> x0, other arithmetic: 7.95 us -> none  [the longest x1 3.15 us: body(): weighted = jnp.where(is_local[:, None], picked * route_weights.reshape(-1...]
  transfers between devices with their start and end apart: 13 -> 0, of which waited for: 8 -> 0; matrix products, arithmetic and copies ran while one was open for 34% -> 0% of each run, Pallas kernels for 0% -> 0%
where the time goes in v1:
time: 198 us; the launch traced here: 195 us
  Pallas kernels  169 us (85%)
  local copies, waits for them, and re-layouts  14 us (7%)
  matrix products  11 us (6%)
    pallas_call x1, Pallas kernels, body(): pl.pallas_call(combine_kernel, out_shape=jax.ShapeDtypeStruct((16, D), BF...  89.7 us
    pallas_call x1, Pallas kernels, body(): pl.pallas_call(gather_kernel, out_shape=(jax.ShapeDtypeStruct((D, 256), B...  79.8 us
    unnamed x20, local copies, waits for them, and re-layouts  13.3 us
    dot_general x1, matrix products, body(): part = jnp.dot(hidden, down, preferred_element_type=F32).astype(BF)  8.83 us

profile of v1, /device:TPU:1, one launch (start us, length us, event | category | flops | bytes accessed | tf_op | source)
XLA Modules:
  0.0 195.2 jit_solution(15405314770643673476)
XLA Ops:
  0.6 0.8 copy.11.ids
  1.4 0.7 copy.12.gain
  2.2 0.0 copy-start.1
  2.2 1.2 copy-done.1
  3.4 0.0 copy-start.2
  3.4 1.2 copy-done.2
  4.6 1.2 copy-done.3
  5.8 0.0 copy-start.4
  5.8 1.0 copy-done.4
  6.9 79.8 %gather.1 = (bf16[2048,256]{1,0:T(8,128)(2,1)S(1)}, bf16[2048,256]{1,0:T(8,128)(2,1)S(1)}, bf16[256,2048]{1,0:T(8,128)(2,1)S(1)}, bf16[8,4,32,2048]{3,2,1,0:T(8,128)(2,1)S(1)}) custom-call(bf16[128,2048]{1,0:T(8,128)(2,1)S(1)} %copy-done.4, s32[128,2]{1,0:T(8,128)S(1)} %copy.11.ids, f32[64,1]{1,0:T(8,128)S(1)} %copy.12.gain, f32[4,64,1024]{2,1,0:T(8,128)S(1)} %copy-done.1, ...), custom_call_target="tpu_custom_call" | custom-call | tf_op jit(solution)/shard_map/gather/pallas_call | solution.py:450
  86.7 0.0 copy-start.5
  86.7 1.9 copy-done.5
  88.6 2.2 %fusion.8 = f32[1024,256]{1,0:T(8,128)} fusion(bf16[1024,2048]{1,0:T(8,128)(2,1)S(1)} %bitcast.15, bf16[2048,256]{1,0:T(8,128)(2,1)S(1)} %get-tuple-element.8), kind=kOutput, calls=%fused_computation.10 | convolution fusion | flops 1073741824 | bytes 6291456 | tf_op jit(solution)/shard_map/dot_general | solution.py:484
  90.8 0.0 copy-start.6
  90.8 8.8 %convolution_convert_fusion = bf16[1024,2048]{1,0:T(8,128)(2,1)} fusion(bf16[256,2048]{1,0:T(8,128)(2,1)S(1)} %get-tuple-element.10, bf16[1024,2048]{1,0:T(8,128)(2,1)} %bitcast.16, bf16[2048,256]{1,0:T(8,128)(2,1)S(1)} %get-tuple-element.9, f32[1024,256]{1,0:T(8,128)} %fusion.8), kind=kOutput, calls=%fused_computation | convolution fusion | flops 2151153664 | bytes 11534336 | tf_op jit(solution)/shard_map/dot_general | solution.py:487
  99.7 0.0 copy-done.6
  99.7 0.1 copy.14.weights
  99.8 0.0 copy-start
  99.8 2.2 %copy-done = bf16[1024,2048]{1,0:T(8,128)(2,1)S(1)} copy-done((bf16[1024,2048]{1,0:T(8,128)(2,1)S(1)}, bf16[1024,2048]{1,0:T(8,128)(2,1)}, u32[]{:S(2)}) %copy-start) | copy-done | bytes 4194328
  102.0 89.7 %combine.1 = bf16[16,2048]{1,0:T(8,128)(2,1)S(1)} custom-call(bf16[8,4,32,2048]{3,2,1,0:T(8,128)(2,1)S(1)} %bitcast.11, s32[128,2]{1,0:T(8,128)S(1)} %copy.11.ids, f32[128,2]{1,0:T(8,128)S(1)} %copy.14.weights), custom_call_target="tpu_custom_call" | custom-call | tf_op jit(solution)/shard_map/combine/pallas_call | solution.py:488
  191.7 1.0 copy.19
  192.6 1.0 copy.20
  193.6 1.0 copy.21
  194.6 0.6 copy.22
  (1 shorter events, 0.0 us)
Async XLA Ops:
  2.2 1.2 copy-start.1
  3.4 1.2 copy-start.2
  4.6 1.2 copy-start.3
  5.8 1.0 copy-start.4
  86.7 1.9 copy-start.5
  90.8 8.8 %copy-start.6 = (f32[128,2]{0,1:T(2,128)S(1)}, f32[128,2]{0,1:T(2,128)}, u32[]{:S(2)}) copy-start(f32[128,2]{0,1:T(2,128)} %param.9) | copy-start | bytes 3076
  99.8 2.2 %copy-start = (bf16[1024,2048]{1,0:T(8,128)(2,1)S(1)}, bf16[1024,2048]{1,0:T(8,128)(2,1)}, u32[]{:S(2)}) copy-start(bf16[1024,2048]{1,0:T(8,128)(2,1)} %convolution_convert_fusion) | copy-start | bytes 12582916

commit v2 on v1

v2 whole, which is shorter than its diff:
```python
import jax
import jax.numpy as jnp
from jax import lax
from jax.experimental import pallas as pl
from jax.experimental.pallas import tpu as pltpu
from jax.sharding import PartitionSpec as P

EXPERTS = 8
SLOTS = 32
TOK = 128
D = 2048
NORM_EPS = 1e-06
MESH = pl.DeviceIdType.MESH
BF = jnp.bfloat16
F32 = jnp.float32


def place():
    g, f, t = lax.axis_index("gr"), lax.axis_index("fs"), lax.axis_index("tp")
    return g, lax.div(f, 8), lax.rem(f, 8), lax.div(t, 2), lax.rem(t, 2)


def dev(g, zl, y, x, c):
    return (g, zl * 8 + y, x * 2 + c)


def signal(sem, where):
    pl.semaphore_signal(sem, inc=1, device_id=where, device_id_type=MESH)


def rcopy(src, dst, ssem, rsem, where):
    return pltpu.make_async_remote_copy(
        src_ref=src, dst_ref=dst, send_sem=ssem, recv_sem=rsem, device_id=where, device_id_type=MESH
    )


def arrived(buf, sem):
    pltpu.make_async_copy(buf, buf, sem).wait()


def home_of(g, el):
    odd = lax.rem(el, 2)
    x1 = 2 * g + lax.div(el, 2)
    return x1, odd, x1 * (1 - odd) + (3 - x1) * odd


def served_by(g, x):
    h = lax.div(x, 2)
    c1 = h + g - 2 * h * g
    return x * (1 - c1) + (3 - x) * c1, c1


def choice_matrix(ids):
    e = lax.axis_index("tp")
    mine = jnp.sum((ids == e).astype(F32), axis=0, keepdims=True)
    mine = jnp.broadcast_to(mine, (SLOTS, TOK))
    row = lax.broadcasted_iota(jnp.int32, (TOK, TOK), 0)
    col = lax.broadcasted_iota(jnp.int32, (TOK, TOK), 1)
    before = (row < col).astype(BF)
    rank = jnp.dot(mine.astype(BF), before, preferred_element_type=F32)
    slot = lax.broadcasted_iota(jnp.int32, (SLOTS, TOK), 0).astype(F32)
    return jnp.where((mine > 0.5) & (jnp.abs(rank - slot) < 0.5), 1.0, 0.0)


def kernel(
    prompt_h, gate_h, up_h, down_h, ids, weights, gain,
    gate_out, up_out, down_out, mixed,
    prompt, gate, up, down, stg, stgd, abuf, dbuf, rows,
    hid, part, keep, got, fin, gotz, sendc, gotc,
    in_s, a_s, a_r, d_s, d_r, b_s, b_r, e_s, e_r, t_s, t_r, y_s, y_r,
    p_s, p_r, z_s, z_r, c_s, c_r,
):
    loads = [
        pltpu.make_async_copy(src, dst, in_s.at[i])
        for i, (src, dst) in enumerate(
            ((prompt_h, prompt), (down_h, down), (gate_h, gate), (up_h, up))
        )
    ]
    for load in loads:
        load.start()
    g, zl, y, x, c = place()
    me_t = x * 2 + c
    barrier = pltpu.get_barrier_semaphore()
    right = dev(g, zl, lax.rem(y + 1, 8), x, c)
    left = dev(g, zl, lax.rem(y + 7, 8), x, c)
    half = lax.div(y, 4)
    x1, c1 = served_by(g, x)
    ge = lax.div(x, 2)
    _, _, xe = home_of(ge, lax.rem(me_t, 4))

    @pl.loop(0, 32)
    def _(i):
        xs, ys = lax.div(i, 8), lax.rem(i, 8)

        @pl.when((xs != x) | (ys != y) | (half != c))
        def _():
            signal(barrier, dev(g, zl, ys, xs, half))

    @pl.loop(0, 8)
    def _(i):
        @pl.when(i != me_t)
        def _():
            signal(barrier, (g, zl * 8 + y, i))

        zs, w = lax.div(i, 2), lax.rem(i, 2)

        @pl.when((ge != g) | (zs != zl) | (xe != x) | (w != c))
        def _():
            signal(barrier, dev(ge, zs, y, xe, w))

    @pl.loop(1, 4)
    def _(j):
        signal(barrier, dev(g, lax.rem(zl + j, 4), y, x, c))

    signal(barrier, right)
    signal(barrier, left)

    choice = choice_matrix(ids[...])
    wslot = jnp.sum(
        choice
        * jnp.sum(jnp.where(ids[...] == me_t, weights[...], 0.0), axis=0, keepdims=True),
        axis=1,
        keepdims=True,
    )
    chosen = choice.astype(BF)
    loads[0].wait()
    xf = prompt[...].astype(F32)
    normed = (xf * lax.rsqrt(jnp.mean(xf * xf, axis=1, keepdims=True) + NORM_EPS)).astype(BF)
    rows[y, zl] = jnp.dot(chosen, normed, preferred_element_type=F32).astype(BF)

    loads[1].wait()

    @pl.loop(0, 4)
    def _(el):
        for h in range(2):
            stgd[el, h] = down[el, h * 128 : (h + 1) * 128, :].astype(BF)

    eye = lax.broadcasted_iota(jnp.int32, (64, 64), 0) == lax.broadcasted_iota(jnp.int32, (64, 64), 1)
    col = jnp.sum(
        jnp.where(eye, jnp.broadcast_to(gain[...], (64, 64)), 0.0), axis=1, keepdims=True
    )
    loads[2].wait()
    loads[3].wait()

    @pl.loop(0, 4)
    def _(el):
        for k in range(4):
            cols = slice(k * 256, (k + 1) * 256)
            stg[0, el, k] = (gate[el, :, cols] * col).astype(BF)
            stg[1, el, k] = (up[el, :, cols] * col).astype(BF)

    same_half = jnp.where(half == c, 1, 0)
    own_b = jnp.where(ge == g, 1, 0) * (1 - c)
    pl.semaphore_wait(barrier, 32 - same_half + 7 + 8 - own_b + 3 + 2)

    def z_send(j):
        to = lax.rem(zl + j, 4)
        return rcopy(rows.at[y, zl], rows.at[y, zl], t_s.at[j], t_r.at[zl], dev(g, to, y, x, c))

    def r_send(s, q):
        at = lax.rem(y - s + 9, 8)
        return rcopy(rows.at[at, q], rows.at[at, q], y_s.at[0, s, q], y_r.at[0, s, q], right)

    def l_send(s, q):
        at = lax.rem(y + s + 7, 8)
        return rcopy(rows.at[at, q], rows.at[at, q], y_s.at[1, s, q], y_r.at[1, s, q], left)

    @pl.loop(1, 4)
    def _(j):
        z_send(j).start()

    def collected(x2):
        x0, c0 = served_by(g, x2)
        return 2 * (x0 - 2 * g) + c0

    def d_parts(i):
        x2, h = lax.rem(x + 1 + lax.div(i, 2), 4), lax.rem(i, 2)
        own = (x2 == x) & (h == c)
        dst = dbuf.at[x, :, pl.ds(pl.multiple_of(c * 256, 256), 256)]
        return own, stgd.at[collected(x2), h], dst, dev(g, zl, y, x2, h)

    @pl.loop(0, 8)
    def _(i):
        own, src, dst, to = d_parts(i)

        @pl.when(own)
        def _():
            pltpu.make_async_copy(src, dst, d_r.at[x]).start()

        @pl.when(jnp.logical_not(own))
        def _():
            rcopy(src, dst, d_s.at[i], d_r.at[x], to).start()

    r_send(1, zl).start()
    l_send(1, zl).start()

    def a_parts(i):
        k, w = lax.rem(y + lax.rem(lax.div(i, 2), 4), 4), lax.rem(i, 2)
        x2 = lax.rem(x + 5 + lax.div(i, 8) - zl, 4)
        el, y2 = collected(x2), 4 * c + k
        own = (x2 == x) & (w == c) & (y2 == y)
        dst = abuf.at[x, pl.ds(pl.multiple_of(y * 64, 64), 64), :]
        return own, stg.at[w, el, k], dst, dev(g, zl, y2, x2, w)

    @pl.loop(0, 32)
    def _(i):
        own, src, dst, to = a_parts(i)

        @pl.when(own)
        def _():
            pltpu.make_async_copy(src, dst, a_r.at[x]).start()

        @pl.when(jnp.logical_not(own))
        def _():
            rcopy(src, dst, a_s.at[i], a_r.at[x], to).start()

    def e_parts(i):
        j, g2 = lax.div(i, 2), lax.rem(g + 1 + i, 2)
        own = (g2 == g) & (x1 == x) & (c1 == c)
        dst = down_out.at[
            pl.ds(pl.multiple_of(c * 128, 128), 128), pl.ds(pl.multiple_of(j * 512, 512), 512)
        ]
        return own, dbuf.at[j], dst, dev(g2, zl, y, x1, c1), e_r.at[c, j]

    def e_start(first):
        @pl.loop(first, first + 4)
        def _(i):
            own, src, dst, to, sem = e_parts(i)

            @pl.when(lax.rem(i, 2) == 0)
            def _():
                arrived(src, d_r.at[lax.div(i, 2)])

            @pl.when(own)
            def _():
                pltpu.make_async_copy(src, dst, sem).start()

            @pl.when(jnp.logical_not(own))
            def _():
                rcopy(src, dst, e_s.at[i], sem, to).start()

    e_start(0)

    def b_parts(i, out):
        xs, g2 = lax.rem(x + 7 - lax.div(i, 2) + zl, 4), lax.rem(g + 1 + i, 2)
        own = (g2 == g) & (xs == zl) & (x1 == x) & (c1 == c)
        dst = out.at[pl.ds(pl.multiple_of(zl * 512, 512), 512), :]
        return own, abuf.at[xs], dst, dev(g2, xs, y, x1, c1)

    def b_step(m):
        xs = lax.rem(x + 7 - m + zl, 4)
        arrived(abuf.at[xs], a_r.at[xs])
        for w, out in ((0, gate_out), (1, up_out)):

            @pl.when(c == w)
            def _():
                @pl.loop(2 * m, 2 * m + 2)
                def _(i):
                    own, src, dst, to = b_parts(i, out)

                    @pl.when(own)
                    def _():
                        pltpu.make_async_copy(src, dst, b_r.at[w, zl]).start()

                    @pl.when(jnp.logical_not(own))
                    def _():
                        rcopy(src, dst, b_s.at[i], b_r.at[w, zl], to).start()

    def nth(j):
        return lax.rem(zl + 4 + j * (1 - 2 * lax.div(zl, 2)), 4)

    for m in range(4):
        b_step(m)
        if m < 3:
            q = nth(m + 1)
            arrived(rows.at[y, q], t_r.at[q])
            r_send(1, q).start()
            l_send(1, q).start()

    e_start(4)

    def ring_step(s):
        @pl.loop(0, 4)
        def _(j):
            q = nth(j)
            arrived(rows.at[lax.rem(y - s + 9, 8), q], y_r.at[0, s - 1, q])
            arrived(rows.at[lax.rem(y + s + 7, 8), q], y_r.at[1, s - 1, q])
            if s < 4:
                r_send(s, q).start()
                l_send(s, q).start()
            else:

                @pl.when(q < 2)
                def _():
                    r_send(s, q).start()

                @pl.when(q >= 2)
                def _():
                    l_send(s, q).start()

    for s in (2, 3, 4):
        ring_step(s)

    far = lax.rem(y + 4, 8)
    for q in range(4):
        arrived(rows.at[far, q], y_r.at[q // 2, 4, q])
    for q in range(4):
        arrived(gate_out.at[q * 512 : (q + 1) * 512, :], b_r.at[0, q])
        arrived(up_out.at[q * 512 : (q + 1) * 512, :], b_r.at[1, q])
    @pl.loop(0, 4)
    def _(i):
        x_in = rows[pl.ds(2 * i, 2)].reshape(8 * SLOTS, D)
        gate_part = jnp.dot(x_in, gate_out[...], preferred_element_type=F32)
        up_part = jnp.dot(x_in, up_out[...], preferred_element_type=F32)
        hid[i] = (gate_part / (1.0 + jnp.exp(-gate_part)) * up_part).astype(BF)

    def target(way, s):
        return lax.rem(y + 5 - s, 8) if way == 0 else lax.rem(y + 3 + s, 8)

    def send(way, s, q, src):
        return rcopy(
            src, got.at[way, s - 1, q], p_s.at[way, s - 1, q], p_r.at[way, s - 1, q], (right, left)[way]
        )

    def first_hand(way, s, q):
        return s == 1 or (s == 2 and q // 2 != way)

    def source(way, s, q):
        if first_hand(way, s, q):
            return part.at[target(way, s), q]
        return keep.at[way, s - 2, q]

    def make(q):
        for h in range(2):
            at = down_out.at[h * 128 : (h + 1) * 128, q * 512 : (q + 1) * 512]
            arrived(at, e_r.at[h, q])

        @pl.loop(0, 4)
        def _(i):
            made = jnp.dot(
                hid[i], down_out[:, q * 512 : (q + 1) * 512], preferred_element_type=F32
            ).astype(BF)
            part[2 * i, q] = made[:128]
            part[2 * i + 1, q] = made[128:]

        send(q // 2, 1, q, source(q // 2, 1, q)).start()
        send(1 - q // 2, 2, q, source(1 - q // 2, 2, q)).start()

    def pass_on(way, s, q):
        arrived(got.at[way, s - 2, q], p_r.at[way, s - 2, q])
        total = part[target(way, s), q].astype(F32) + got[way, s - 2, q].astype(F32)
        keep[way, s - 2, q] = total.astype(BF)
        send(way, s, q, source(way, s, q)).start()

    for q in (0, 1, 2, 3):
        make(q)
    for s, order in ((2, (0, 1)), (3, (2, 3, 0, 1)), (4, (2, 0, 3, 1))):
        for j in order:
            for way in range(2):
                pass_on(way, s, (j + 2 * way) % 4)

    def f_send(q, j):
        to = lax.rem(zl + j, 4)
        src = fin.at[q, pl.ds(pl.multiple_of(to * 32, 32), 32), :]
        return rcopy(src, gotz.at[q, zl], z_s.at[q, j], z_r.at[q, zl], dev(g, to, y, x, c))

    def finish(q):
        for way in range(2):
            arrived(got.at[way, 3, q], p_r.at[way, 3, q])
        total = part[y, q].astype(F32) + got[0, 3, q].astype(F32) + got[1, 3, q].astype(F32)
        fin[q] = total.astype(BF)

        @pl.loop(1, 4)
        def _(j):
            f_send(q, j).start()

    def c_send(q, j):
        t = lax.rem(me_t + j, 8)
        return rcopy(
            sendc.at[q, t], gotc.at[q, me_t], c_s.at[q, j], c_r.at[q, me_t], (g, zl * 8 + y, t)
        )

    def spread(q):
        out = fin[q, pl.ds(pl.multiple_of(zl * 32, 32), 32), :].astype(F32)
        for j in range(1, 4):
            k = lax.rem(zl + j, 4)
            arrived(gotz.at[q, k], z_r.at[q, k])
            out = out + gotz[q, k].astype(F32)
        term = (out * wslot).astype(BF)
        wide = lax.dot_general(
            chosen, term, (((0,), (0,)), ((), ())), preferred_element_type=F32
        ).astype(BF)
        for t in range(8):
            sendc[q, t] = wide[t * 16 : (t + 1) * 16, :]

        @pl.loop(1, 8)
        def _(j):
            c_send(q, j).start()

    def settle(q):
        total = sendc[q, me_t].astype(F32)
        for j in range(1, 8):
            t = lax.rem(me_t + j, 8)
            arrived(gotc.at[q, t], c_r.at[q, t])
            total = total + gotc[q, t].astype(F32)
        mixed[:, q * 512 : (q + 1) * 512] = total.astype(BF)

    @pl.loop(1, 4)
    def _(j):
        z_send(j).wait_send()

    @pl.loop(0, 8)
    def _(i):
        own, src, dst, to = d_parts(i)

        @pl.when(jnp.logical_not(own))
        def _():
            rcopy(src, dst, d_s.at[i], d_r.at[x], to).wait_send()

    @pl.loop(0, 32)
    def _(i):
        own, src, dst, to = a_parts(i)

        @pl.when(jnp.logical_not(own))
        def _():
            rcopy(src, dst, a_s.at[i], a_r.at[x], to).wait_send()

    @pl.loop(0, 8)
    def _(i):
        own, src, dst, to, sem = e_parts(i)

        @pl.when(jnp.logical_not(own))
        def _():
            rcopy(src, dst, e_s.at[i], sem, to).wait_send()

    @pl.loop(0, 8)
    def _(i):
        own, src, dst, to = b_parts(i, gate_out)

        @pl.when(jnp.logical_not(own))
        def _():
            rcopy(src, dst, b_s.at[i], b_r.at[0, zl], to).wait_send()

    for s in (1, 2, 3):

        @pl.loop(0, 4)
        def _(q):
            r_send(s, q).wait_send()
            l_send(s, q).wait_send()

    for q in range(2):
        r_send(4, q).wait_send()
        l_send(4, q + 2).wait_send()

    for s in (1, 2, 3):
        for q in range(4):
            for way in range(2):
                if s > 1 or q // 2 == way:
                    send(way, s, q, source(way, s, q)).wait_send()

    for q in (0, 2, 1, 3):
        finish(q)
    for q in (0, 2, 1, 3):
        spread(q)
    for q in (0, 2, 1, 3):
        settle(q)

    for q in range(4):
        for way in range(2):
            send(way, 4, q, source(way, 4, q)).wait_send()

        @pl.loop(1, 4)
        def _(j):
            f_send(q, j).wait_send()

        @pl.loop(1, 8)
        def _(j):
            c_send(q, j).wait_send()


VM = pl.BlockSpec(memory_space=pltpu.VMEM)
HB = pl.BlockSpec(memory_space=pltpu.MemorySpace.HBM)
DMA = pltpu.SemaphoreType.DMA


def body(prompt, expert_ids, route_weights, gate_master, up_master, down_master, ffn_gain):
    gate, up, down, mixed = pl.pallas_call(
        kernel,
        out_shape=(
            jax.ShapeDtypeStruct((D, 256), BF),
            jax.ShapeDtypeStruct((D, 256), BF),
            jax.ShapeDtypeStruct((256, D), BF),
            jax.ShapeDtypeStruct((16, D), BF),
        ),
        in_specs=[HB] * 4 + [VM] * 3,
        out_specs=(VM,) * 4,
        scratch_shapes=[
            pltpu.VMEM((TOK, D), BF),
            pltpu.VMEM((4, 64, 1024), F32),
            pltpu.VMEM((4, 64, 1024), F32),
            pltpu.VMEM((4, 256, 256), F32),
            pltpu.VMEM((2, 4, 4, 64, 256), BF),
            pltpu.VMEM((4, 2, 128, 256), BF),
            pltpu.VMEM((4, 512, 256), BF),
            pltpu.VMEM((4, 128, 512), BF),
            pltpu.VMEM((8, 4, SLOTS, D), BF),
            pltpu.VMEM((4, 256, 256), BF),
            pltpu.VMEM((8, 4, 128, 512), BF),
            pltpu.VMEM((2, 3, 4, 128, 512), BF),
            pltpu.VMEM((2, 4, 4, 128, 512), BF),
            pltpu.VMEM((4, 128, 512), BF),
            pltpu.VMEM((4, 4, SLOTS, 512), BF),
            pltpu.VMEM((4, 8, 16, 512), BF),
            pltpu.VMEM((4, 8, 16, 512), BF),
            DMA((4,)),
            DMA((32,)),
            DMA((4,)),
            DMA((8,)),
            DMA((4,)),
            DMA((8,)),
            DMA((2, 4)),
            DMA((8,)),
            DMA((2, 4)),
            DMA((4,)),
            DMA((4,)),
            DMA((2, 5, 4)),
            DMA((2, 5, 4)),
            DMA((2, 4, 4)),
            DMA((2, 4, 4)),
            DMA((4, 4)),
            DMA((4, 4)),
            DMA((4, 8)),
            DMA((4, 8)),
        ],
        compiler_params=pltpu.CompilerParams(
            collective_id=0, has_side_effects=True, vmem_limit_bytes=36 << 20
        ),
        name="serve",
    )(
        *(
            pltpu.with_memory_space_constraint(v, pltpu.MemorySpace.HBM)
            for v in (prompt, gate_master, up_master, down_master)
        ),
        expert_ids.T, route_weights.T, ffn_gain[None],
    )
    return gate[None], up[None], down[None], mixed


def solution(mesh):
    return jax.shard_map(
        body,
        mesh=mesh,
        in_specs=(
            P(("gr", "fs"), None),
            P(("gr", "fs"), None),
            P(("gr", "fs"), None),
            P("gr", "fs", "tp"),
            P("gr", "fs", "tp"),
            P("gr", "fs", "tp"),
            P("fs"),
        ),
        out_specs=(
            P("tp", None, "fs"),
            P("tp", None, "fs"),
            P("tp", "fs", None),
            P(("gr", "fs", "tp"), None),
        ),
        check_vma=False,
    )
```

time: 198 us -> 158 us (0.80); the launches traced: 195 us -> 158 us
  Pallas kernels: 169 us -> 153 us
  matrix products: 11 us -> 0 us
  local copies, waits for them, and re-layouts: 14 us -> 4.21 us
    pallas_call x2 -> x1, Pallas kernels: 169 us -> 153 us  [body(): pl.pallas_call(kernel, out_shape=(jax.ShapeDtypeStruct((D, 256), BF), jax...]
    dot_general x2 -> x0, matrix products: 11 us -> none  [the longest x1 8.83 us: body(): part = jnp.dot(hidden, down, preferred_element_type=F32).astype(BF)]
    unnamed x20 -> x10, local copies, waits for them, and re-layouts: 13.3 us -> 4.21 us
where the time goes in v2:
time: 158 us
  Pallas kernels  153 us (97%)
  local copies, waits for them, and re-layouts  4.21 us (3%)
    pallas_call x1, Pallas kernels, body(): pl.pallas_call(kernel, out_shape=(jax.ShapeDtypeStruct((D, 256), BF), jax...  153 us
    unnamed x10, local copies, waits for them, and re-layouts  4.21 us

profile of v2, /device:TPU:1, one launch (start us, length us, event | category | flops | bytes accessed | tf_op | source)
XLA Modules:
  0.0 157.6 jit_solution(2842682585880531161)
XLA Ops:
  0.6 0.0 copy-start.1
  0.6 0.0 copy-start
  0.7 0.0 copy-start.2
  0.7 0.7 copy-done.1
  1.3 0.0 copy-done
  1.3 0.0 copy-done.2
  1.3 152.7 %serve.1 = (bf16[2048,256]{1,0:T(8,128)(2,1)S(1)}, bf16[2048,256]{1,0:T(8,128)(2,1)S(1)}, bf16[256,2048]{1,0:T(8,128)(2,1)S(1)}, bf16[16,2048]{1,0:T(8,128)(2,1)S(1)}) custom-call(bf16[128,2048]{1,0:T(8,128)(2,1)} %prompt_h.1, f32[4,64,1024]{2,1,0:T(8,128)} %gate_h.1, f32[4,64,1024]{2,1,0:T(8,128)} %up_h.1, f32[4,256,256]{2,1,0:T(8,128)} %down_h.1, ...), custom_call_target="tpu_custom_call" | custom-call | tf_op jit(solution)/shard_map/serve/pallas_call | solution.py:487
  154.1 1.0 copy.15
  155.1 1.0 copy.16
  156.0 1.0 copy.17
  157.0 0.6 copy.18
Async XLA Ops:
  0.6 0.7 copy-start.1
  0.6 0.7 copy-start
  0.7 0.7 copy-start.2

commit v3 on v2

--- a/solution.py
+++ b/solution.py
@@ -66,7 +66,7 @@
     prompt_h, gate_h, up_h, down_h, ids, weights, gain,
     gate_out, up_out, down_out, mixed,
     prompt, gate, up, down, stg, stgd, abuf, dbuf, rows,
-    hid, part, keep, got, fin, gotz, sendc, gotc,
+    acc, hid, part, keep, got, fin, gotz, sendc, gotc,
     in_s, a_s, a_r, d_s, d_r, b_s, b_r, e_s, e_r, t_s, t_r, y_s, y_r,
     p_s, p_r, z_s, z_r, c_s, c_r,
 ):
@@ -242,7 +242,7 @@
     e_start(0)
 
     def b_parts(i, out):
-        xs, g2 = lax.rem(x + 7 - lax.div(i, 2) + zl, 4), lax.rem(g + 1 + i, 2)
+        xs, g2 = lax.rem(x + 7 - lax.div(i, 2) + zl, 4), lax.rem(i, 2)
         own = (g2 == g) & (xs == zl) & (x1 == x) & (c1 == c)
         dst = out.at[pl.ds(pl.multiple_of(zl * 512, 512), 512), :]
         return own, abuf.at[xs], dst, dev(g2, xs, y, x1, c1)
@@ -304,15 +304,25 @@
     far = lax.rem(y + 4, 8)
     for q in range(4):
         arrived(rows.at[far, q], y_r.at[q // 2, 4, q])
-    for q in range(4):
-        arrived(gate_out.at[q * 512 : (q + 1) * 512, :], b_r.at[0, q])
-        arrived(up_out.at[q * 512 : (q + 1) * 512, :], b_r.at[1, q])
-    @pl.loop(0, 4)
-    def _(i):
-        x_in = rows[pl.ds(2 * i, 2)].reshape(8 * SLOTS, D)
-        gate_part = jnp.dot(x_in, gate_out[...], preferred_element_type=F32)
-        up_part = jnp.dot(x_in, up_out[...], preferred_element_type=F32)
-        hid[i] = (gate_part / (1.0 + jnp.exp(-gate_part)) * up_part).astype(BF)
+    for m in range(4):
+        q = lax.rem(zl + m - xe + 5, 4)
+        at = pl.ds(pl.multiple_of(q * 512, 512), 512)
+        arrived(gate_out.at[at, :], b_r.at[0, q])
+        arrived(up_out.at[at, :], b_r.at[1, q])
+
+        @pl.loop(0, 4)
+        def _(i):
+            x_in = rows[pl.ds(2 * i, 2), :, :, at].reshape(8 * SLOTS, 512)
+            gate_part = jnp.dot(x_in, gate_out[at, :], preferred_element_type=F32)
+            up_part = jnp.dot(x_in, up_out[at, :], preferred_element_type=F32)
+            if m > 0:
+                gate_part = gate_part + acc[0, i]
+                up_part = up_part + acc[1, i]
+            if m < 3:
+                acc[0, i] = gate_part
+                acc[1, i] = up_part
+            else:
+                hid[i] = (gate_part / (1.0 + jnp.exp(-gate_part)) * up_part).astype(BF)
 
     def target(way, s):
         return lax.rem(y + 5 - s, 8) if way == 0 else lax.rem(y + 3 + s, 8)
@@ -362,7 +372,7 @@
     def f_send(q, j):
         to = lax.rem(zl + j, 4)
         src = fin.at[q, pl.ds(pl.multiple_of(to * 32, 32), 32), :]
-        return rcopy(src, gotz.at[q, zl], z_s.at[q, j], z_r.at[q, zl], dev(g, to, y, x, c))
+        return rcopy(src, gotz.at[q, zl], z_s.at[q], z_r.at[q], dev(g, to, y, x, c))
 
     def finish(q):
         for way in range(2):
@@ -377,15 +387,14 @@
     def c_send(q, j):
         t = lax.rem(me_t + j, 8)
         return rcopy(
-            sendc.at[q, t], gotc.at[q, me_t], c_s.at[q, j], c_r.at[q, me_t], (g, zl * 8 + y, t)
+            sendc.at[q, t], gotc.at[q, me_t], c_s.at[q], c_r.at[q], (g, zl * 8 + y, t)
         )
 
     def spread(q):
         out = fin[q, pl.ds(pl.multiple_of(zl * 32, 32), 32), :].astype(F32)
+        arrived(gotz.at[q, 0:3], z_r.at[q])
         for j in range(1, 4):
-            k = lax.rem(zl + j, 4)
-            arrived(gotz.at[q, k], z_r.at[q, k])
-            out = out + gotz[q, k].astype(F32)
+            out = out + gotz[q, lax.rem(zl + j, 4)].astype(F32)
         term = (out * wslot).astype(BF)
         wide = lax.dot_general(
             chosen, term, (((0,), (0,)), ((), ())), preferred_element_type=F32
@@ -398,11 +407,10 @@
             c_send(q, j).start()
 
     def settle(q):
+        arrived(gotc.at[q, 0:7], c_r.at[q])
         total = sendc[q, me_t].astype(F32)
         for j in range(1, 8):
-            t = lax.rem(me_t + j, 8)
-            arrived(gotc.at[q, t], c_r.at[q, t])
-            total = total + gotc[q, t].astype(F32)
+            total = total + gotc[q, lax.rem(me_t + j, 8)].astype(F32)
         mixed[:, q * 512 : (q + 1) * 512] = total.astype(BF)
 
     @pl.loop(1, 4)
@@ -462,20 +470,14 @@
         finish(q)
     for q in (0, 2, 1, 3):
         spread(q)
-    for q in (0, 2, 1, 3):
-        settle(q)
-
     for q in range(4):
         for way in range(2):
             send(way, 4, q, source(way, 4, q)).wait_send()
-
-        @pl.loop(1, 4)
-        def _(j):
-            f_send(q, j).wait_send()
-
-        @pl.loop(1, 8)
-        def _(j):
-            c_send(q, j).wait_send()
+        arrived(fin.at[q, 0:96, :], z_s.at[q])
+    for q in (0, 2, 1, 3):
+        settle(q)
+    for q in range(4):
+        arrived(sendc.at[q, 0:7], c_s.at[q])
 
 
 VM = pl.BlockSpec(memory_space=pltpu.VMEM)
@@ -483,8 +485,16 @@
 DMA = pltpu.SemaphoreType.DMA
 
 
+def store_kernel(*refs):
+    copies = [pltpu.make_async_copy(refs[i], refs[4 + i], refs[8].at[i]) for i in range(4)]
+    for one in copies:
+        one.start()
+    for one in copies:
+        one.wait()
+
+
 def body(prompt, expert_ids, route_weights, gate_master, up_master, down_master, ffn_gain):
-    gate, up, down, mixed = pl.pallas_call(
+    made = pl.pallas_call(
         kernel,
         out_shape=(
             jax.ShapeDtypeStruct((D, 256), BF),
@@ -504,6 +514,7 @@
             pltpu.VMEM((4, 512, 256), BF),
             pltpu.VMEM((4, 128, 512), BF),
             pltpu.VMEM((8, 4, SLOTS, D), BF),
+            pltpu.VMEM((2, 4, 256, 256), F32),
             pltpu.VMEM((4, 256, 256), BF),
             pltpu.VMEM((8, 4, 128, 512), BF),
             pltpu.VMEM((2, 3, 4, 128, 512), BF),
@@ -527,10 +538,10 @@
             DMA((2, 5, 4)),
             DMA((2, 4, 4)),
             DMA((2, 4, 4)),
-            DMA((4, 4)),
-            DMA((4, 4)),
-            DMA((4, 8)),
-            DMA((4, 8)),
+            DMA((4,)),
+            DMA((4,)),
+            DMA((4,)),
+            DMA((4,)),
         ],
         compiler_params=pltpu.CompilerParams(
             collective_id=0, has_side_effects=True, vmem_limit_bytes=36 << 20
@@ -543,6 +554,15 @@
         ),
         expert_ids.T, route_weights.T, ffn_gain[None],
     )
+    gate, up, down, mixed = pl.pallas_call(
+        store_kernel,
+        out_shape=tuple(jax.ShapeDtypeStruct(v.shape, BF) for v in made),
+        in_specs=[VM] * 4,
+        out_specs=(HB,) * 4,
+        scratch_shapes=[DMA((4,))],
+        compiler_params=pltpu.CompilerParams(vmem_limit_bytes=8 << 20),
+        name="store",
+    )(*made)
     return gate[None], up[None], down[None], mixed
 
 

time: 158 us -> 154 us (0.975)
  local copies, waits for them, and re-layouts: 4.21 us -> 0.67 us
    unnamed x10 -> x6, local copies, waits for them, and re-layouts: 4.21 us -> 0.67 us
    pallas_call x1, Pallas kernels: 153 us -> 150 us  [body(): pl.pallas_call(kernel, out_shape=(jax.ShapeDtypeStruct((D, 256), BF), jax...]
    pallas_call x0 -> x1, Pallas kernels: none -> 1.7 us  [body(): pl.pallas_call(store_kernel, out_shape=tuple((jax.ShapeDtypeStruct(v.shap...]
where the time goes in v3:
time: 154 us
  Pallas kernels  152 us (99%)
    pallas_call x1, Pallas kernels, body(): pl.pallas_call(kernel, out_shape=(jax.ShapeDtypeStruct((D, 256), BF), jax...  150 us

profile of v3, /device:TPU:1, one launch (start us, length us, event | category | flops | bytes accessed | tf_op | source)
XLA Modules:
  0.0 153.5 jit_solution(17161528905198512088)
XLA Ops:
  0.6 0.0 copy-start.1
  0.6 0.0 copy-start
  0.7 0.0 copy-start.2
  0.7 0.7 copy-done.1
  1.3 0.0 copy-done
  1.3 0.0 copy-done.2
  1.3 150.5 %serve.1 = (bf16[2048,256]{1,0:T(8,128)(2,1)S(1)}, bf16[2048,256]{1,0:T(8,128)(2,1)S(1)}, bf16[256,2048]{1,0:T(8,128)(2,1)S(1)}, bf16[16,2048]{1,0:T(8,128)(2,1)S(1)}) custom-call(bf16[128,2048]{1,0:T(8,128)(2,1)} %prompt_h.1, f32[4,64,1024]{2,1,0:T(8,128)} %gate_h.1, f32[4,64,1024]{2,1,0:T(8,128)} %up_h.1, f32[4,256,256]{2,1,0:T(8,128)} %down_h.1, ...), custom_call_target="tpu_custom_call" | custom-call | tf_op jit(solution)/shard_map/serve/pallas_call | solution.py:497
  151.8 1.7 %store.1 = (bf16[2048,256]{1,0:T(8,128)(2,1)}, bf16[2048,256]{1,0:T(8,128)(2,1)}, bf16[256,2048]{1,0:T(8,128)(2,1)}, bf16[16,2048]{1,0:T(8,128)(2,1)}) custom-call(bf16[2048,256]{1,0:T(8,128)(2,1)S(1)} %get-tuple-element.12.refs_0_, bf16[2048,256]{1,0:T(8,128)(2,1)S(1)} %get-tuple-element.13.refs_1_, bf16[256,2048]{1,0:T(8,128)(2,1)S(1)} %get-tuple-element.14.refs_2_, ...), custom_call_target="tpu_custom_call" | custom-call | tf_op jit(solution)/shard_map/store/pallas_call | solution.py:557
Async XLA Ops:
  0.6 0.7 copy-start.1
  0.6 0.7 copy-start
  0.7 0.7 copy-start.2

commit v4 on v3

--- a/solution.py
+++ b/solution.py
@@ -215,7 +215,7 @@
             rcopy(src, dst, a_s.at[i], a_r.at[x], to).start()
 
     def e_parts(i):
-        j, g2 = lax.div(i, 2), lax.rem(g + 1 + i, 2)
+        j, g2 = lax.div(i, 2), lax.rem(i, 2)
         own = (g2 == g) & (x1 == x) & (c1 == c)
         dst = down_out.at[
             pl.ds(pl.multiple_of(c * 128, 128), 128), pl.ds(pl.multiple_of(j * 512, 512), 512)
@@ -369,8 +369,7 @@
             for way in range(2):
                 pass_on(way, s, (j + 2 * way) % 4)
 
-    def f_send(q, j):
-        to = lax.rem(zl + j, 4)
+    def f_send(q, to):
         src = fin.at[q, pl.ds(pl.multiple_of(to * 32, 32), 32), :]
         return rcopy(src, gotz.at[q, zl], z_s.at[q], z_r.at[q], dev(g, to, y, x, c))
 
@@ -380,9 +379,11 @@
         total = part[y, q].astype(F32) + got[0, 3, q].astype(F32) + got[1, 3, q].astype(F32)
         fin[q] = total.astype(BF)
 
-        @pl.loop(1, 4)
-        def _(j):
-            f_send(q, j).start()
+        @pl.loop(0, 4)
+        def _(to):
+            @pl.when(to != zl)
+            def _():
+                f_send(q, to).start()
 
     def c_send(q, j):
         t = lax.rem(me_t + j, 8)

time: 154 us -> 154 us (level)
  no operation moved by 1% of the time
where the time goes in v4:
time: 154 us; the launch traced here: 153 us
  Pallas kernels  152 us (99%)
    pallas_call x1, Pallas kernels, body(): pl.pallas_call(kernel, out_shape=(jax.ShapeDtypeStruct((D, 256), BF), jax...  150 us

profile of v4, /device:TPU:1, one launch (start us, length us, event | category | flops | bytes accessed | tf_op | source)
XLA Modules:
  0.0 153.5 jit_solution(6980146035093320797)
XLA Ops:
  0.6 0.0 copy-start.1
  0.6 0.0 copy-start
  0.7 0.0 copy-start.2
  0.7 0.7 copy-done.1
  1.3 0.0 copy-done
  1.3 0.0 copy-done.2
  1.3 150.4 %serve.1 = (bf16[2048,256]{1,0:T(8,128)(2,1)S(1)}, bf16[2048,256]{1,0:T(8,128)(2,1)S(1)}, bf16[256,2048]{1,0:T(8,128)(2,1)S(1)}, bf16[16,2048]{1,0:T(8,128)(2,1)S(1)}) custom-call(bf16[128,2048]{1,0:T(8,128)(2,1)} %prompt_h.1, f32[4,64,1024]{2,1,0:T(8,128)} %gate_h.1, f32[4,64,1024]{2,1,0:T(8,128)} %up_h.1, f32[4,256,256]{2,1,0:T(8,128)} %down_h.1, ...), custom_call_target="tpu_custom_call" | custom-call | tf_op jit(solution)/shard_map/serve/pallas_call | solution.py:498
  151.8 1.7 %store.1 = (bf16[2048,256]{1,0:T(8,128)(2,1)}, bf16[2048,256]{1,0:T(8,128)(2,1)}, bf16[256,2048]{1,0:T(8,128)(2,1)}, bf16[16,2048]{1,0:T(8,128)(2,1)}) custom-call(bf16[2048,256]{1,0:T(8,128)(2,1)S(1)} %get-tuple-element.12.refs_0_, bf16[2048,256]{1,0:T(8,128)(2,1)S(1)} %get-tuple-element.13.refs_1_, bf16[256,2048]{1,0:T(8,128)(2,1)S(1)} %get-tuple-element.14.refs_2_, ...), custom_call_target="tpu_custom_call" | custom-call | tf_op jit(solution)/shard_map/store/pallas_call | solution.py:558
Async XLA Ops:
  0.6 0.7 copy-start.1
  0.6 0.7 copy-start
  0.7 0.7 copy-start.2
